TPU v7x, 32 devices: a whole 2x2x4 slice. The times are simulated.
32 devices in a mesh: ep: 16 (over z, y, x), tp: 2 (over core).
Axes of the slice: x: 2, y: 2, z: 4, core: 2. Of those that a mesh axis runs over, the one named last changes fastest.
Arguments:
- tokens: bfloat16 [384, 2048], P('ep'), may hold values from -6 to 6
- attn_gain: float32 [2048], replicated, may hold values from 0.1 to 1.9
- w_query: bfloat16 [2048, 1024], P(None, 'tp'), may hold values from -0.125 to 0.125
- w_key: bfloat16 [2048, 1024], P(None, 'tp'), may hold values from -0.125 to 0.125
- w_value: bfloat16 [2048, 1024], P(None, 'tp'), may hold values from -0.125 to 0.125
- w_zgate: bfloat16 [2048, 1024], P(None, 'tp'), may hold values from -0.125 to 0.125
- w_decay: bfloat16 [2048, 8], P(None, 'tp'), may hold values from -0.125 to 0.125
- w_beta: bfloat16 [2048, 8], P(None, 'tp'), may hold values from -0.125 to 0.125
- decay_rate: float32 [8], P('tp'), may hold values from 0.05 to 2
- decay_bias: float32 [8], P('tp'), may hold values from -3 to 3
- state: float32 [384, 8, 128, 128], P('ep', 'tp'), may hold values from -2 to 2
- out_gain: float32 [128], replicated, may hold values from 0.1 to 1.9
- w_out: bfloat16 [1024, 2048], P('tp'), may hold values from -0.1875 to 0.1875
- ffn_gain: float32 [2048], replicated, may hold values from 0.1 to 1.9
- expert_gate: bfloat16 [16, 2048, 512], P('ep', None, 'tp'), may hold values from -0.125 to 0.125
- expert_up: bfloat16 [16, 2048, 512], P('ep', None, 'tp'), may hold values from -0.125 to 0.125
- expert_down: bfloat16 [16, 512, 2048], P('ep', 'tp'), may hold values from -0.25 to 0.25
- routes: int32 [384, 2], P('ep'), may hold values from 0 to 15, all different within a row; in each aligned block of 24 rows (0 to 23, 24 to 47, ...) at most 6 rows name the same one
- route_weight: float32 [384, 2], P('ep'), may hold values from 0.2 to 1
Outputs:
- layer_out: bfloat16 [384, 2048], P('ep', 'tp')
- new_state: float32 [384, 8, 128, 128], P('ep', 'tp')
Inputs may be any that keep to these rules, and one draw needn't show every extreme that they name: `routes`: the 2 entries of a row differ. Among the rows of one index of ep (aligned blocks of 24 rows) no expert is named more than 6 times, a bound that some block reaches.
All inputs are finite; a program needn't handle non-finite values.
Results may differ from a plain program's by a relative error of at most 0.014.
Values may be sent and summed in bfloat16 or wider, within the bound.
A program may use at most 128 MiB of HBM per device.

v0:
```python
import jax
import jax.numpy as jnp
from jax import lax
from jax.sharding import PartitionSpec as P

EPS = 1e-06


def rms_scale(rows, gain):
    return rows * lax.rsqrt(jnp.mean(rows * rows, axis=-1, keepdims=True) + EPS) * gain


def unit_rows(rows):
    return rows * lax.rsqrt(jnp.sum(rows * rows, axis=-1, keepdims=True) + EPS)


def per_device(
    tokens,
    attn_gain,
    w_query,
    w_key,
    w_value,
    w_zgate,
    w_decay,
    w_beta,
    decay_rate,
    decay_bias,
    state,
    out_gain,
    w_out,
    ffn_gain,
    expert_gate,
    expert_up,
    expert_down,
    routes,
    route_weight,
):
    seqs, width = tokens.shape
    heads = state.shape[1]
    head_dim = state.shape[2]
    top = routes.shape[1]
    resid_in = tokens.astype(jnp.float32)
    normed = rms_scale(resid_in, attn_gain).astype(jnp.bfloat16)

    def project(weight):
        return jnp.dot(normed, weight, preferred_element_type=jnp.float32).astype(jnp.bfloat16)

    def heads_of(raw):
        return raw.reshape(seqs, heads, head_dim).astype(jnp.float32)

    query = unit_rows(jax.nn.silu(heads_of(project(w_query)))) * head_dim ** (-0.5)
    key = unit_rows(jax.nn.silu(heads_of(project(w_key))))
    value = jax.nn.silu(heads_of(project(w_value)))
    zmul = jax.nn.silu(heads_of(project(w_zgate)))
    fade = jnp.exp(-decay_rate * jax.nn.softplus(project(w_decay).astype(jnp.float32) + decay_bias))
    beta = jax.nn.sigmoid(project(w_beta).astype(jnp.float32))
    predicted = jnp.einsum("shkv,shk->shv", state, key, precision=lax.Precision.HIGHEST)
    written = beta[..., None] * (value - fade[..., None] * predicted)
    new_state = fade[..., None, None] * state + key[..., :, None] * written[..., None, :]
    read = jnp.einsum("shkv,shk->shv", new_state, query, precision=lax.Precision.HIGHEST)
    heads_out = (
        (rms_scale(read, out_gain) * zmul).astype(jnp.bfloat16).reshape(seqs, heads * head_dim)
    )
    partial_value = jnp.dot(heads_out, w_out, preferred_element_type=jnp.float32)
    mixed = lax.psum(partial_value.astype(jnp.bfloat16), "tp").astype(jnp.float32)
    resid = resid_in + mixed
    moe_in = rms_scale(resid, ffn_gain).astype(jnp.bfloat16)
    experts = lax.axis_size("ep")
    cap = max(2, 2 * seqs * top // experts)
    flat_routes = routes.reshape(-1)
    onehot = (flat_routes[:, None] == jnp.arange(experts, dtype=jnp.int32)[None, :]).astype(
        jnp.int32
    )
    before = jnp.cumsum(onehot, axis=0) - onehot
    slot = jnp.sum(before * onehot, axis=1)
    place = flat_routes * cap + slot
    pick = (place[:, None] == jnp.arange(experts * cap, dtype=jnp.int32)[None, :]).astype(
        jnp.bfloat16
    )
    columns = width // lax.axis_size("tp")
    own_part = lax.dynamic_slice_in_dim(moe_in, lax.axis_index("tp") * columns, columns, 1)
    spread = jnp.repeat(own_part, top, axis=0)
    outgoing = jnp.dot(pick.T, spread, preferred_element_type=jnp.float32).astype(jnp.bfloat16)
    outgoing = outgoing.reshape(experts, 1, cap, columns)
    arrived = lax.all_gather(
        lax.all_to_all(outgoing, "ep", split_axis=0, concat_axis=1, tiled=True),
        "tp",
        axis=3,
        tiled=True,
    )
    flat_rows = arrived.reshape(-1, arrived.shape[-1])
    gate = jnp.dot(flat_rows, expert_gate[0], preferred_element_type=jnp.float32)
    up = jnp.dot(flat_rows, expert_up[0], preferred_element_type=jnp.float32)
    hidden = (jax.nn.silu(gate) * up).astype(jnp.bfloat16)
    term = jnp.dot(hidden, expert_down[0], preferred_element_type=jnp.float32)
    terms = term.reshape(arrived.shape[:-1] + (term.shape[-1],))
    summed = lax.psum_scatter(terms.astype(jnp.bfloat16), "tp", scatter_dimension=3, tiled=True)
    returned = lax.all_to_all(summed, "ep", split_axis=1, concat_axis=0, tiled=True)
    returned = returned.reshape(experts * cap, columns)
    per_route = jnp.dot(pick, returned, preferred_element_type=jnp.float32).reshape(
        seqs, top, columns
    )
    combined = jnp.sum(per_route * route_weight[..., None], axis=1)
    own_resid = lax.dynamic_slice_in_dim(resid, lax.axis_index("tp") * columns, columns, 1)
    layer_out = (own_resid + combined).astype(jnp.bfloat16)
    return (layer_out, new_state)


def solution(mesh):
    in_specs = (
        P("ep", None),
        P(),
        P(None, "tp"),
        P(None, "tp"),
        P(None, "tp"),
        P(None, "tp"),
        P(None, "tp"),
        P(None, "tp"),
        P("tp"),
        P("tp"),
        P("ep", "tp", None, None),
        P(),
        P("tp", None),
        P(),
        P("ep", None, "tp"),
        P("ep", None, "tp"),
        P("ep", "tp", None),
        P("ep", None),
        P("ep", None),
    )
    out_specs = (P("ep", "tp"), P("ep", "tp", None, None))
    return jax.shard_map(
        per_device, mesh=mesh, in_specs=in_specs, out_specs=out_specs, check_vma=False
    )
```

profile of v0, /device:TPU:0, one launch (start us, length us, event | category | flops | bytes accessed | tf_op | source)
XLA Modules:
  0.0 115.3 jit_solution(10898759450930380615)
XLA Ops:
  7.2 0.0 copy-start
  7.2 0.0 copy-start.2
  7.2 0.0 copy-start.5
  7.2 0.0 all-reduce.2.cloned.1.call-start
  7.3 1.2 %fusion.18 = f32[24]{0:T(128)S(1)} fusion(bf16[24,2048]{1,0:T(8,128)(2,1)} %param.19), kind=kLoop, calls=%fused_computation.33 | loop fusion | flops 147432 | bytes 98400 | tf_op jit(solution)/shard_map/reduce_sum | solution.py:10
  8.4 0.0 copy-start.11
  8.5 2.1 %fusion.6 = f32[24,512]{1,0:T(8,128)S(1)} fusion(bf16[2048,512]{1,0:T(8,128)(2,1)} %param.22, bf16[24,2048]{1,0:T(8,128)(2,1)} %param.19, f32[2048]{0:T(1024)} %param.20, f32[24]{0:T(128)S(1)} %add_rsqrt_fusion.4), kind=kOutput, calls=%fused_computation.16 | convolution fusion | flops 50552832 | bytes 2252896 | tf_op jit(solution)/shard_map/dot_general | solution.py:46
  10.6 0.1 multiply_reduce_fusion.3
  10.7 0.1 broadcast_multiply_fusion
  10.8 0.0 copy-done.12
  10.9 0.2 fusion.34
  11.1 0.1 copy.48
  11.2 2.0 %fusion.5 = f32[24,512]{1,0:T(8,128)S(1)} fusion(bf16[2048,512]{1,0:T(8,128)(2,1)} %param.23, bf16[24,2048]{1,0:T(8,128)(2,1)S(1)} %copy-done.2, f32[2048]{0:T(1024)S(1)} %copy-done.5, f32[24]{0:T(128)S(1)} %add_rsqrt_fusion.4), kind=kOutput, calls=%fused_computation.14 | convolution fusion | flops 50552832 | bytes 2252896 | tf_op jit(solution)/shard_map/dot_general | solution.py:46
  13.3 0.2 fusion.13
  13.5 0.1 copy.49
  13.6 8.1 %fusion.41 = f32[24,4,1,128]{3,2,1,0:T(1,128)S(1)} fusion(f32[24,4,128,1]{2,3,1,0:T(1,128)S(1)} %bitcast.48, f32[24,4,128,128]{3,2,1,0:T(8,128)} %param.29), kind=kOutput, calls=%fused_computation.73 | convolution fusion | flops 18874368 | bytes 6389760 | tf_op jit(solution)/shard_map/shkv,shk->shv/dot_general | solution.py:57
  21.7 0.1 fusion.24
  21.8 0.0 copy-start.3
  21.8 3.9 %multiply_add_fusion = f32[24,4,128,128]{3,2,1,0:T(8,128)} fusion(f32[24,4,128,128]{3,2,1,0:T(8,128)S(1)} %copy-done.1, f32[24,4,128]{2,1,0:T(4,128)S(1)} %fusion.24, f32[24,4,128]{2,1,0:T(4,128)S(1)} %broadcast_multiply_fusion, f32[24,4]{1,0:T(8,128)S(1)} %copy.48), kind=kLoop, calls=%fused_computation | loop fusion | flops 4718592 | bytes 12681600 | tf_op jit(solution)/shard_map/add | solution.py:59
  25.7 0.4 fusion.4
  26.2 0.1 multiply_reduce_fusion.2
  26.3 0.1 multiply_multiply_fusion
  26.4 0.0 copy-start.4
  26.4 7.5 %fusion.42 = f32[24,4,1,128]{3,2,1,0:T(1,128)S(1)} fusion(f32[24,4,128,128]{3,2,1,0:T(8,128)} %multiply_add_fusion, f32[24,4,128,1]{2,3,1,0:T(1,128)S(1)} %bitcast.51), kind=kOutput, calls=%fused_computation.74 | convolution fusion | flops 18874368 | bytes 6389760 | tf_op jit(solution)/shard_map/shkv,shk->shv/dot_general | solution.py:60
  33.9 0.1 multiply_reduce_fusion.1
  34.1 0.0 copy-done.4
  34.1 0.0 copy-start.6
  34.1 0.0 copy-start.7
  34.1 0.4 fusion.3
  34.6 0.0 copy-done.9
  34.6 0.1 fusion.25
  34.7 1.0 convolution_convert_fusion.1
  35.7 0.0 all-reduce.2.cloned.1.call-update
  35.8 0.0 reduce-scatter.2.cloned.1.call-start
  35.8 0.0 copy-done.6
  35.8 0.1 copy.51
  35.9 0.1 eq.50
  36.0 0.1 fusion.28
  36.1 0.1 reduce_window_sum.11
  36.2 0.2 select_reduce_fusion
  36.4 0.0 copy-done.7
  36.4 20.1 %all-reduce.2.cloned.1.call-done = bf16[24,2048]{1,0:T(8,128)(2,1)} async-done(((bf16[24,2048]{1,0:T(8,128)(2,1)}), bf16[24,2048]{1,0:T(8,128)(2,1)}) %all-reduce.2.cloned.1.call-update) | async-done | bytes 98320 | tf_op jit(solution)/shard_map/psum | solution.py:65
  56.5 1.0 multiply_reduce_fusion
  57.5 0.1 multiply_convert_fusion
  57.6 0.1 broadcast_in_dim.2
  57.7 0.3 convolution_convert_fusion.2
  58.0 0.1 reshape.136
  58.1 16.9 %all_to_all.21 = bf16[16,1,6,1024]{3,2,1,0:T(8,128)(2,1)S(1)} all-to-all(bf16[16,1,6,1024]{3,2,1,0:T(8,128)(2,1)S(1)} %bitcast.47), channel_id=1, replica_groups=mesh['ep'=16,'tp'=2] {'ep'}, dimensions={0} | all-to-all | bytes 393216 | tf_op jit(solution)/shard_map/all_to_all | solution.py:86
  75.0 2.2 %all-gather = bf16[16,1,6,2048]{3,2,1,0:T(8,128)(2,1)S(1)} all-gather(bf16[16,1,6,1024]{3,2,1,0:T(8,128)(2,1)S(1)} %all_to_all.21), channel_id=2, replica_groups=mesh['ep'=16,'tp'=2] {'tp'}, dimensions={3}, use_global_device_ids=true | all-gather | bytes 589824 | tf_op jit(solution)/shard_map/all_gather | solution.py:85
  77.2 0.1 reshape.137
  77.3 1.5 %fusion.16 = f32[96,256]{1,0:T(8,128)S(1)} fusion(bf16[96,2048]{1,0:T(8,128)(2,1)S(1)} %reshape.137, bf16[1,2048,256]{2,1,0:T(8,128)(2,1)} %param.33), kind=kOutput, calls=%fused_computation.28 | convolution fusion | flops 100663296 | bytes 1540096 | tf_op jit(solution)/shard_map/dot_general | solution.py:92
  78.9 1.5 %fusion.2 = bf16[96,256]{1,0:T(8,128)(2,1)S(1)} fusion(bf16[96,2048]{1,0:T(8,128)(2,1)S(1)} %reshape.137, bf16[1,2048,256]{2,1,0:T(8,128)(2,1)} %param.34, f32[96,256]{1,0:T(8,128)S(1)} %fusion.16), kind=kOutput, calls=%fused_computation.8 | convolution fusion | flops 100810752 | bytes 1589248 | tf_op jit(solution)/shard_map/dot_general | solution.py:93
  80.4 0.0 copy-start.8
  80.5 2.3 %fusion = bf16[1,16,6,2048]{3,1,2,0:T(8,128)(2,1)} fusion(bf16[1,256,2048]{2,1,0:T(8,128)(2,1)} %param.35, bf16[16,6,256]{2,1,0:T(8,128)(2,1)S(1)} %dot_general.56), kind=kOutput, calls=%fused_computation.2 | convolution fusion | flops 100859904 | bytes 1490944 | tf_op jit(solution)/shard_map/dot_general | solution.py:95
  82.7 0.0 reduce-scatter.2.cloned.1.call-update
  82.8 5.9 %reduce-scatter.2.cloned.1.call-done = bf16[1,16,6,1024]{3,1,2,0:T(8,128)(2,1)} async-done(((bf16[1,16,6,2048]{3,1,2,0:T(8,128)(2,1)}), bf16[1,16,6,1024]{3,1,2,0:T(8,128)(2,1)}) %reduce-scatter.2.cloned.1.call-update) | async-done | bytes 196624 | tf_op jit(solution)/shard_map/reduce_scatter | solution.py:97
  88.6 1.7 %copy.55 = bf16[1,16,6,1024]{3,2,0,1:T(8,128)(2,1)} copy(bf16[1,16,6,1024]{3,1,2,0:T(8,128)(2,1)} %reduce-scatter.2.cloned.1.call-done) | data formatting | bytes 393216 | tf_op jit(solution)/shard_map/reduce_scatter | solution.py:97
  90.4 6.7 %all-to-all-start.1 = ((bf16[1,16,6,1024]{3,2,0,1:T(8,128)(2,1)}), bf16[1,16,6,1024]{3,2,0,1:T(8,128)(2,1)S(1)}, u32[]{:S(2)}, u32[]{:S(2)}) async-start(bf16[1,16,6,1024]{3,2,0,1:T(8,128)(2,1)} %copy.55), calls=%async_computation.2 | async-start | bytes 524288 | tf_op jit(solution)/shard_map/all_to_all | solution.py:98
  97.1 0.1 reduce_sum.70
  97.2 0.1 copy.52
  97.3 10.2 %all-to-all-done.1 = bf16[1,16,6,1024]{3,2,0,1:T(8,128)(2,1)S(1)} async-done(((bf16[1,16,6,1024]{3,2,0,1:T(8,128)(2,1)}), bf16[1,16,6,1024]{3,2,0,1:T(8,128)(2,1)S(1)}, u32[]{:S(2)}, u32[]{:S(2)}) %all-to-all-start.1) | async-done | bytes 196640 | tf_op jit(solution)/shard_map/all_to_all | solution.py:98
  107.5 0.1 reshape.150
  107.6 0.2 fusion.1
  107.8 0.6 add_convert_fusion
  (29 shorter events, 0.2 us)
Async XLA Ops:
  7.2 27.5 %copy-start = (bf16[512,2048]{1,0:T(8,128)(2,1)S(1)}, bf16[512,2048]{1,0:T(8,128)(2,1)}, u32[]{:S(2)}) copy-start(bf16[512,2048]{1,0:T(8,128)(2,1)} %param.31) | copy-start | bytes 6291460
  7.2 3.7 %copy-start.2 = (bf16[24,2048]{1,0:T(8,128)(2,1)S(1)}, bf16[24,2048]{1,0:T(8,128)(2,1)}, u32[]{:S(2)}) copy-start(bf16[24,2048]{1,0:T(8,128)(2,1)} %param.19) | copy-start | bytes 294916
  7.2 3.7 %copy-start.5 = (f32[2048]{0:T(1024)S(1)}, f32[2048]{0:T(1024)}, u32[]{:S(2)}) copy-start(f32[2048]{0:T(1024)} %param.20) | copy-start | bytes 24580
  7.2 3.6 %copy-start.12 = (f32[4]{0:T(128)S(1)}, f32[4]{0:T(128)}, u32[]{:S(2)}) copy-start(f32[4]{0:T(128)} %param.27) | copy-start | bytes 52
  7.2 3.7 %copy-start.10 = (bf16[2048,4]{0,1:T(4,128)(2,1)S(1)}, bf16[2048,4]{0,1:T(4,128)(2,1)}, u32[]{:S(2)}) copy-start(bf16[2048,4]{0,1:T(4,128)(2,1)} %param.25) | copy-start | bytes 49156
  7.2 3.7 %copy-start.13 = (f32[4]{0:T(128)S(1)}, f32[4]{0:T(128)}, u32[]{:S(2)}) copy-start(f32[4]{0:T(128)} %param.28) | copy-start | bytes 52
  7.2 49.2 %all-reduce.2.cloned.1.call-start = ((), (), s32[]{:S(2)}) async-start(), calls=%async_computation.3 | async-start | bytes 196608 | tf_op jit(solution)/shard_map/psum | solution.py:65
  8.4 4.8 %copy-start.11 = (bf16[2048,4]{0,1:T(4,128)(2,1)S(1)}, bf16[2048,4]{0,1:T(4,128)(2,1)}, u32[]{:S(2)}) copy-start(bf16[2048,4]{0,1:T(4,128)(2,1)} %param.26) | copy-start | bytes 49156
  13.6 8.2 %copy-start.1 = (f32[24,4,128,128]{3,2,1,0:T(8,128)S(1)}, f32[24,4,128,128]{3,2,1,0:T(8,128)}, u32[]{:S(2)}) copy-start(f32[24,4,128,128]{3,2,1,0:T(8,128)} %param.29) | copy-start | bytes 18874372
  21.8 3.9 %copy-start.3 = (bf16[2048,512]{1,0:T(8,128)(2,1)S(1)}, bf16[2048,512]{1,0:T(8,128)(2,1)}, u32[]{:S(2)}) copy-start(bf16[2048,512]{1,0:T(8,128)(2,1)} %param.21) | copy-start | bytes 6291460
  26.4 7.7 %copy-start.4 = (bf16[2048,512]{1,0:T(8,128)(2,1)S(1)}, bf16[2048,512]{1,0:T(8,128)(2,1)}, u32[]{:S(2)}) copy-start(bf16[2048,512]{1,0:T(8,128)(2,1)} %param.24) | copy-start | bytes 6291460
  33.9 0.7 copy-start.9
  34.1 1.7 %copy-start.6 = (s32[24,2]{0,1:T(2,128)S(1)}, s32[24,2]{0,1:T(2,128)}, u32[]{:S(2)}) copy-start(s32[24,2]{0,1:T(2,128)} %param.36) | copy-start | bytes 580
  34.1 2.3 %copy-start.7 = (f32[2048]{0:T(1024)S(1)}, f32[2048]{0:T(1024)}, u32[]{:S(2)}) copy-start(f32[2048]{0:T(1024)} %param.32) | copy-start | bytes 24580
  35.8 52.9 %reduce-scatter.2.cloned.1.call-start = ((), (), s32[]{:S(2)}) async-start(), calls=%async_computation.4 | async-start | bytes 589824 | tf_op jit(solution)/shard_map/reduce_scatter | solution.py:97
  80.4 27.2 %copy-start.8 = (f32[24,2]{0,1:T(2,128)S(1)}, f32[24,2]{0,1:T(2,128)}, u32[]{:S(2)}) copy-start(f32[24,2]{0,1:T(2,128)} %param.37) | copy-start | bytes 580
  90.4 17.1 %all-to-all-start.1 = ((bf16[1,16,6,1024]{3,2,0,1:T(8,128)(2,1)}), bf16[1,16,6,1024]{3,2,0,1:T(8,128)(2,1)S(1)}, u32[]{:S(2)}, u32[]{:S(2)}) async-start(bf16[1,16,6,1024]{3,2,0,1:T(8,128)(2,1)} %copy.55), calls=%async_computation.2 | async-start | bytes 524288 | tf_op jit(solution)/shard_map/all_to_all | solution.py:98
Sparse Core Ops, SparseCore 0:
  35.9 20.5 all-reduce.1
  82.9 5.7 reduce-scatter.1
where the time goes:
time: 116 us; the launch traced here: 115 us
  waiting for transfers between devices  36.2 us (31%)
  matrix products  28 us (24%)
  blocking collectives  19.1 us (16%)
  between operations  14.4 us (12%)
  other arithmetic  7.91 us (7%)
  starting transfers between devices  6.81 us (6%)
  local copies, waits for them, and re-layouts  2.86 us (2%)
    psum x1, waiting for transfers between devices, per_device(): lax.psum(partial_value.astype(jnp.bfloat16), 'tp').astype(jnp.float32)  20.1 us
    all_to_all x1, blocking collectives, per_device(): lax.all_to_all(outgoing, 'ep', split_axis=0, concat_axis=1, tiled=True)  16.9 us
    all_to_all x1, waiting for transfers between devices, per_device(): lax.all_to_all(summed, 'ep', split_axis=1, concat_axis=0, tiled=True)  10.2 us
    dot_general x1, matrix products, per_device(): jnp.einsum('shkv,shk->shv', state, key, precision=lax.Precision.HIGHEST)  8.09 us
    dot_general x1, matrix products, per_device(): jnp.einsum('shkv,shk->shv', new_state, query, precision=lax.Precision.HIG...  7.54 us
    all_to_all x1, starting transfers between devices, per_device(): lax.all_to_all(summed, 'ep', split_axis=1, concat_axis=0, tiled=True)  6.73 us
    reduce_scatter x1, waiting for transfers between devices, per_device(): lax.psum_scatter(terms.astype(jnp.bfloat16), 'tp', scatter_dimension=3, t...  5.89 us
    dot_general x6, matrix products, project(): jnp.dot(normed, weight, preferred_element_type=jnp.float32)  5.45 us
  transfers between devices with their start and end apart: 3, of which 3 were waited for; matrix products, arithmetic and copies ran while one was open for 1% of the time, Pallas kernels for 0%

commit v1 on v0

v1 whole, which is shorter than its diff:
```python
import functools

import jax
import jax.numpy as jnp
from jax import lax
from jax.experimental import pallas as pl
from jax.experimental.pallas import tpu as pltpu
from jax.sharding import PartitionSpec as P

EPS = 1e-06
F32 = jnp.float32
BF16 = jnp.bfloat16
ANY = pl.BlockSpec(memory_space=pl.ANY)
VMEM = pl.BlockSpec(memory_space=pltpu.VMEM)


def rms_scale(rows, gain):
    return rows * lax.rsqrt(jnp.mean(rows * rows, axis=-1, keepdims=True) + EPS) * gain


def unit_rows(rows):
    return rows * lax.rsqrt(jnp.sum(rows * rows, axis=-1, keepdims=True) + EPS)


def silu(x):
    return x * jax.nn.sigmoid(x)


def mixer_kernel(
    step,
    tokens,
    gain,
    wq,
    wk,
    wv,
    wz,
    wd,
    wb,
    rate,
    bias,
    state,
    out_gain,
    heads_out,
    new_state,
    wbuf,
    st,
    ns,
    kq,
    vals,
    zbuf,
    fades,
    betas,
    dots,
    reads,
    w_sem,
    in_sem,
    out_sem,
):
    seqs, heads, dim, _ = st.shape
    chunks = seqs // step

    def w_copy(n):
        return pltpu.make_async_copy((wq, wk, wv, wz)[n], wbuf.at[n], w_sem.at[n])

    def in_copy(c):
        rows = pl.ds(c * step, step)
        return pltpu.make_async_copy(state.at[rows], st.at[rows], in_sem.at[c])

    def out_copy(c):
        rows = pl.ds(c * step, step)
        return pltpu.make_async_copy(ns.at[rows], new_state.at[rows], out_sem.at[c])

    for n in range(4):
        w_copy(n).start()
    for c in range(chunks):
        in_copy(c).start()

    normed = rms_scale(tokens[...].astype(F32), gain[...]).astype(BF16)

    def rounded(weight):
        return jnp.dot(normed, weight, preferred_element_type=F32).astype(BF16).astype(F32)

    xa = rounded(wd[...]) + bias[...]
    fade = jnp.exp(-rate[...] * (jnp.maximum(xa, 0.0) + jnp.log1p(jnp.exp(-jnp.abs(xa)))))
    beta = jax.nn.sigmoid(rounded(wb[...]))
    for h in range(heads):
        fades[:, h, :] = jnp.broadcast_to(fade[:, h : h + 1], (seqs, dim))
        betas[:, h, :] = jnp.broadcast_to(beta[:, h : h + 1], (seqs, dim))
    w_copy(0).wait()
    raw_q = rounded(wbuf[0])
    w_copy(1).wait()
    raw_k = rounded(wbuf[1])
    for h in range(heads):
        cols = slice(h * dim, (h + 1) * dim)
        query = unit_rows(silu(raw_q[:, cols])) * dim ** (-0.5)
        key = unit_rows(silu(raw_k[:, cols]))
        kq[:, h, :] = key
        kq[:, heads + h, :] = query
        dots[:, h, :] = jnp.broadcast_to(jnp.sum(key * query, axis=-1, keepdims=True), (seqs, dim))
    w_copy(2).wait()
    value = silu(rounded(wbuf[2]))
    for h in range(heads):
        vals[:, h, :] = value[:, h * dim : (h + 1) * dim]
    w_copy(3).wait()
    zbuf[...] = silu(rounded(wbuf[3]))

    def one_chunk(c, carry):
        in_copy(c).wait()
        for i in range(step):
            s = c * step + i
            turned = kq[s].T
            fs, bs, vs, ds = fades[s], betas[s], vals[s], dots[s]
            for h in range(heads):
                block = st[s, h]
                kc = jnp.broadcast_to(turned[:, h : h + 1], (dim, dim))
                qc = jnp.broadcast_to(turned[:, heads + h : heads + h + 1], (dim, dim))
                f = fs[h : h + 1]
                pred = jnp.sum(block * kc, axis=0, keepdims=True)
                proj = jnp.sum(block * qc, axis=0, keepdims=True)
                written = bs[h : h + 1] * (vs[h : h + 1] - f * pred)
                ns[s, h] = f * block + kc * written
                reads[s, pl.ds(h, 1)] = f * proj + written * ds[h : h + 1]
        out_copy(c).start()
        return carry

    lax.fori_loop(0, chunks, one_chunk, 0)
    for h in range(heads):
        cols = slice(h * dim, (h + 1) * dim)
        heads_out[:, cols] = (rms_scale(reads[:, h, :], out_gain[...]) * zbuf[:, cols]).astype(BF16)
    for c in range(chunks):
        out_copy(c).wait()


def expert_kernel(
    n_ep,
    n_tp,
    top,
    cap,
    groups,
    tokens,
    heads_out,
    w_out,
    ffn_gain,
    w_gate,
    w_up,
    w_down,
    routes,
    weights,
    out,
    wo,
    wg,
    wu,
    wdn,
    part_out,
    part_in,
    resid,
    moe,
    disp,
    arrived,
    acc_g,
    acc_u,
    other,
    other_in,
    mine,
    ret_out,
    ret_in,
    w_sem,
    part_sem,
    go_send,
    go_recv,
    fw_send,
    fw_recv,
    half_send,
    half_recv,
    back_send,
    back_recv,
):
    seqs, width = tokens.shape
    cols = width // n_tp
    e = lax.axis_index("ep")
    t = lax.axis_index("tp")
    u = n_tp - 1 - t

    def peer(i):
        return lax.rem(e + i, n_ep)

    def source(i):
        return lax.rem(e + n_ep - i, n_ep)

    partner = {"ep": e, "tp": u}
    mesh_ids = pl.DeviceIdType.MESH
    barrier = pltpu.get_barrier_semaphore()
    pl.semaphore_signal(barrier, inc=1, device_id=partner, device_id_type=mesh_ids)

    def greet(i, carry):
        pl.semaphore_signal(barrier, inc=1, device_id={"ep": peer(i), "tp": t}, device_id_type=mesh_ids)
        return carry

    lax.fori_loop(1, n_ep, greet, 0)

    loads = [
        pltpu.make_async_copy(src, dst, w_sem.at[n])
        for n, (src, dst) in enumerate(
            ((w_out, wo), (w_gate.at[0], wg), (w_up.at[0], wu), (w_down.at[0], wdn))
        )
    ]
    for load in loads:
        load.start()

    lower = (
        lax.broadcasted_iota(jnp.int32, (seqs, seqs), 1)
        < lax.broadcasted_iota(jnp.int32, (seqs, seqs), 0)
    ).astype(BF16)
    picks = []
    taken = jnp.zeros((1, n_ep), F32)
    for j in range(top):
        route = routes[:, j : j + 1]
        hot = lax.broadcasted_iota(jnp.int32, (seqs, n_ep), 1) == route
        hot_f = hot.astype(F32)
        before = jnp.dot(lower, hot_f.astype(BF16), preferred_element_type=F32) + taken
        slot = jnp.sum(before * hot_f, axis=1, keepdims=True).astype(jnp.int32)
        taken = taken + jnp.sum(hot_f, axis=0, keepdims=True)
        place = route * cap + slot
        picks.append(
            (lax.broadcasted_iota(jnp.int32, (seqs, n_ep * cap), 1) == place).astype(F32)
        )
    spread = sum(picks[1:], picks[0]).T.astype(BF16)

    loads[0].wait()
    part_out[...] = jnp.dot(heads_out[...], wo[...], preferred_element_type=F32).astype(BF16)
    pl.semaphore_wait(barrier, n_ep)

    swap = pltpu.make_async_remote_copy(
        src_ref=part_out,
        dst_ref=part_in,
        send_sem=part_sem.at[0],
        recv_sem=part_sem.at[1],
        device_id=partner,
        device_id_type=mesh_ids,
    )
    swap.start()
    swap.wait()
    rows = tokens[...].astype(F32) + (part_out[...].astype(F32) + part_in[...].astype(F32))
    resid[...] = rows
    moe[...] = rms_scale(rows, ffn_gain[...]).astype(BF16)
    own = pl.ds(pl.multiple_of(t * cols, 128), cols)
    far = pl.ds(pl.multiple_of(u * cols, 128), cols)
    going = jnp.dot(spread, moe[:, own], preferred_element_type=F32)
    disp[...] = going.reshape(n_ep, cap, cols).astype(BF16)

    def go(i):
        return pltpu.make_async_remote_copy(
            src_ref=disp.at[peer(i)],
            dst_ref=arrived.at[t, e],
            send_sem=go_send.at[i],
            recv_sem=go_recv.at[i],
            device_id={"ep": peer(i), "tp": t},
            device_id_type=mesh_ids,
        )

    def forward(i):
        s = source(i)
        return pltpu.make_async_remote_copy(
            src_ref=arrived.at[t, s],
            dst_ref=arrived.at[t, s],
            send_sem=fw_send.at[i],
            recv_sem=fw_recv.at[i],
            device_id=partner,
            device_id_type=mesh_ids,
        )

    def go_start(i, carry):
        go(i).start()
        return carry

    lax.fori_loop(1, n_ep, go_start, 0)
    arrived[t, e] = disp[e]
    forward(0).start()

    def pass_on(i, carry):
        go(i).wait_recv()
        forward(i).start()
        return carry

    lax.fori_loop(1, n_ep, pass_on, 0)
    loads[1].wait()
    loads[2].wait()

    def half(which):
        got = arrived[which].astype(F32).reshape(n_ep * cap, cols).astype(BF16)
        part = pl.ds(pl.multiple_of(which * cols, 128), cols)
        return (
            jnp.dot(got, wg[part, :], preferred_element_type=F32),
            jnp.dot(got, wu[part, :], preferred_element_type=F32),
        )

    acc_g[...], acc_u[...] = half(t)

    def fw_done(i, carry):
        forward(i).wait_recv()
        return carry

    lax.fori_loop(0, n_ep, fw_done, 0)
    more_g, more_u = half(u)
    hidden = (silu(acc_g[...] + more_g) * (acc_u[...] + more_u)).astype(BF16)
    loads[3].wait()

    size = n_ep // groups

    def give(g):
        span = pl.ds(g * size, size)
        return pltpu.make_async_remote_copy(
            src_ref=other.at[span],
            dst_ref=other_in.at[span],
            send_sem=half_send.at[g],
            recv_sem=half_recv.at[g],
            device_id=partner,
            device_id_type=mesh_ids,
        )

    def back(s):
        i = lax.rem(e + n_ep - s, n_ep)
        return pltpu.make_async_remote_copy(
            src_ref=ret_out.at[s],
            dst_ref=ret_in.at[e],
            send_sem=back_send.at[i],
            recv_sem=back_recv.at[i],
            device_id={"ep": s, "tp": t},
            device_id_type=mesh_ids,
        )

    for g in range(groups):
        rows_g = hidden[g * size * cap : (g + 1) * size * cap]
        term = jnp.dot(rows_g, wdn[:, far], preferred_element_type=F32)
        other[pl.ds(g * size, size)] = term.reshape(size, cap, cols).astype(BF16)
        give(g).start()
    term = jnp.dot(hidden, wdn[:, own], preferred_element_type=F32)
    mine[...] = term.reshape(n_ep, cap, cols).astype(BF16)
    for g in range(groups):
        span = pl.ds(g * size, size)
        give(g).wait_recv()
        both = mine[span].astype(F32) + other_in[span].astype(F32)
        ret_out[span] = both.astype(BF16)

        def back_start(s, carry):
            @pl.when(s != e)
            def _():
                back(s).start()

            return carry

        lax.fori_loop(g * size, (g + 1) * size, back_start, 0)
    ret_in[e] = ret_out[e]

    def back_done(i, carry):
        back(source(i)).wait_recv()
        return carry

    lax.fori_loop(1, n_ep, back_done, 0)
    returned = ret_in[...].astype(F32).reshape(n_ep * cap, cols).astype(BF16)
    total = resid[:, own]
    combined = None
    for j in range(top):
        found = jnp.dot(picks[j].astype(BF16), returned, preferred_element_type=F32)
        term = found * weights[:, j : j + 1]
        combined = term if combined is None else combined + term
    out[...] = (total + combined).astype(BF16)

    forward(0).wait_send()

    def sent(i, carry):
        go(i).wait_send()
        forward(i).wait_send()
        back(source(i)).wait_send()
        return carry

    lax.fori_loop(1, n_ep, sent, 0)
    for g in range(groups):
        give(g).wait_send()


def per_device(
    n_ep,
    n_tp,
    tokens,
    attn_gain,
    w_query,
    w_key,
    w_value,
    w_zgate,
    w_decay,
    w_beta,
    decay_rate,
    decay_bias,
    state,
    out_gain,
    w_out,
    ffn_gain,
    expert_gate,
    expert_up,
    expert_down,
    routes,
    route_weight,
):
    seqs, width = tokens.shape
    heads, dim = state.shape[1], state.shape[2]
    top = routes.shape[1]
    inner = heads * dim
    step = 2 if seqs % 2 == 0 else 1
    chunks = seqs // step
    heads_out, new_state = pl.pallas_call(
        functools.partial(mixer_kernel, step),
        out_shape=(
            jax.ShapeDtypeStruct((seqs, inner), BF16),
            jax.ShapeDtypeStruct(state.shape, F32),
        ),
        in_specs=[VMEM, VMEM, ANY, ANY, ANY, ANY, VMEM, VMEM, VMEM, VMEM, ANY, VMEM],
        out_specs=(VMEM, ANY),
        scratch_shapes=[
            pltpu.VMEM((4, width, inner), BF16),
            pltpu.VMEM(state.shape, F32),
            pltpu.VMEM(state.shape, F32),
            pltpu.VMEM((seqs, 2 * heads, dim), F32),
            pltpu.VMEM((seqs, heads, dim), F32),
            pltpu.VMEM((seqs, inner), F32),
            pltpu.VMEM((seqs, heads, dim), F32),
            pltpu.VMEM((seqs, heads, dim), F32),
            pltpu.VMEM((seqs, heads, dim), F32),
            pltpu.VMEM((seqs, heads, dim), F32),
            pltpu.SemaphoreType.DMA((4,)),
            pltpu.SemaphoreType.DMA((chunks,)),
            pltpu.SemaphoreType.DMA((chunks,)),
        ],
        compiler_params=pltpu.CompilerParams(vmem_limit_bytes=48 * 1024 * 1024),
        name="mixer",
    )(
        tokens,
        attn_gain.reshape(1, width),
        w_query,
        w_key,
        w_value,
        w_zgate,
        w_decay,
        w_beta,
        decay_rate.reshape(1, heads),
        decay_bias.reshape(1, heads),
        state,
        out_gain.reshape(1, dim),
    )

    cap = -(-max(2, 2 * seqs * top // n_ep) // 8) * 8
    cols = width // n_tp
    ff = expert_gate.shape[2]
    groups = 4 if n_ep % 4 == 0 else 1
    slots = (n_ep, cap, cols)
    dma = pltpu.SemaphoreType.DMA
    layer_out = pl.pallas_call(
        functools.partial(expert_kernel, n_ep, n_tp, top, cap, groups),
        out_shape=jax.ShapeDtypeStruct((seqs, cols), BF16),
        in_specs=[VMEM, VMEM, ANY, VMEM, ANY, ANY, ANY, VMEM, VMEM],
        out_specs=VMEM,
        scratch_shapes=[
            pltpu.VMEM((inner, width), BF16),
            pltpu.VMEM((width, ff), BF16),
            pltpu.VMEM((width, ff), BF16),
            pltpu.VMEM((ff, width), BF16),
            pltpu.VMEM((seqs, width), BF16),
            pltpu.VMEM((seqs, width), BF16),
            pltpu.VMEM((seqs, width), F32),
            pltpu.VMEM((seqs, width), BF16),
            pltpu.VMEM(slots, BF16),
            pltpu.VMEM((n_tp,) + slots, BF16),
            pltpu.VMEM((n_ep * cap, ff), F32),
            pltpu.VMEM((n_ep * cap, ff), F32),
            pltpu.VMEM(slots, BF16),
            pltpu.VMEM(slots, BF16),
            pltpu.VMEM(slots, BF16),
            pltpu.VMEM(slots, BF16),
            pltpu.VMEM(slots, BF16),
            dma((4,)),
            dma((2,)),
            dma((n_ep,)),
            dma((n_ep,)),
            dma((n_ep,)),
            dma((n_ep,)),
            dma((groups,)),
            dma((groups,)),
            dma((n_ep,)),
            dma((n_ep,)),
        ],
        compiler_params=pltpu.CompilerParams(
            collective_id=0, has_side_effects=True, vmem_limit_bytes=48 * 1024 * 1024
        ),
        name="experts",
    )(
        tokens,
        heads_out,
        w_out,
        ffn_gain.reshape(1, width),
        expert_gate,
        expert_up,
        expert_down,
        routes,
        route_weight,
    )
    return (layer_out, new_state)


def solution(mesh):
    in_specs = (
        P("ep", None),
        P(),
        P(None, "tp"),
        P(None, "tp"),
        P(None, "tp"),
        P(None, "tp"),
        P(None, "tp"),
        P(None, "tp"),
        P("tp"),
        P("tp"),
        P("ep", "tp", None, None),
        P(),
        P("tp", None),
        P(),
        P("ep", None, "tp"),
        P("ep", None, "tp"),
        P("ep", "tp", None),
        P("ep", None),
        P("ep", None),
    )
    out_specs = (P("ep", "tp"), P("ep", "tp", None, None))
    body = functools.partial(per_device, mesh.shape["ep"], mesh.shape["tp"])
    return jax.shard_map(body, mesh=mesh, in_specs=in_specs, out_specs=out_specs, check_vma=False)
```

time: 116 us -> 51.8 us (0.45)
  Pallas kernels: 0 us -> 37.3 us
  waiting for transfers between devices: 36.2 us -> 0 us
  matrix products: 28 us -> 0 us
  blocking collectives: 19.1 us -> 0 us
  between operations: 14.4 us -> 0.7 us
  local copies, waits for them, and re-layouts: 2.86 us -> 13.3 us
  other arithmetic: 7.91 us -> 0 us
  starting transfers between devices: 6.81 us -> 0 us
    pallas_call x0 -> x2, Pallas kernels: none -> 37.3 us  [the longest x1 25.8 us: per_device(): pl.pallas_call(functools.partial(expert_kernel, n_ep, n_tp, top, cap, gro...]
    dot_general x14 -> x0, matrix products: 28 us -> none  [the longest x1 8.09 us: per_device(): jnp.einsum('shkv,shk->shv', state, key, precision=lax.Precision.HIGHEST)]
    psum x1 -> x0, waiting for transfers between devices: 20.1 us -> none  [per_device(): lax.psum(partial_value.astype(jnp.bfloat16), 'tp').astype(jnp.float32)]
    all_to_all x1 -> x0, blocking collectives: 16.9 us -> none  [per_device(): lax.all_to_all(outgoing, 'ep', split_axis=0, concat_axis=1, tiled=True)]
    unnamed x29 -> x35, local copies, waits for them, and re-layouts: 0.2 us -> 13.3 us
    all_to_all x1 -> x0, waiting for transfers between devices: 10.2 us -> none  [per_device(): lax.all_to_all(summed, 'ep', split_axis=1, concat_axis=0, tiled=True)]
    all_to_all x1 -> x0, starting transfers between devices: 6.73 us -> none  [per_device(): lax.all_to_all(summed, 'ep', split_axis=1, concat_axis=0, tiled=True)]
    reduce_scatter x1 -> x0, waiting for transfers between devices: 5.89 us -> none  [per_device(): lax.psum_scatter(terms.astype(jnp.bfloat16), 'tp', scatter_dimension=3, t...]
  transfers between devices with their start and end apart: 3 -> 0, of which waited for: 3 -> 0; matrix products, arithmetic and copies ran while one was open for 1% -> 0% of each run, Pallas kernels for 0% -> 0%
where the time goes in v1:
time: 51.8 us; the launch traced here: 51.3 us
  Pallas kernels  37.3 us (72%)
  local copies, waits for them, and re-layouts  13.3 us (26%)
  between operations  0.7 us (1%)
    pallas_call x1, Pallas kernels, per_device(): pl.pallas_call(functools.partial(expert_kernel, n_ep, n_tp, top, cap, gro...  25.8 us
    unnamed x35, local copies, waits for them, and re-layouts  13.3 us
    pallas_call x1, Pallas kernels, per_device(): pl.pallas_call(functools.partial(mixer_kernel, step), out_shape=(jax.Shap...  11.5 us

profile of v1, /device:TPU:0, one launch (start us, length us, event | category | flops | bytes accessed | tf_op | source)
XLA Modules:
  0.0 51.3 jit_solution(970442847241091125)
XLA Ops:
  0.6 1.0 %copy.21.wd = bf16[2048,4]{1,0:T(8,128)(2,1)S(1)} copy(bf16[2048,4]{0,1:T(4,128)(2,1)} %param.25) | data formatting | bytes 32768 | tf_op args[6]
  1.7 1.0 %copy.22.wb = bf16[2048,4]{1,0:T(8,128)(2,1)S(1)} copy(bf16[2048,4]{0,1:T(4,128)(2,1)} %param.26) | data formatting | bytes 32768 | tf_op args[7]
  2.7 0.0 copy-start
  2.7 1.6 %copy-done = bf16[2048,512]{1,0:T(8,128)(2,1)S(1)} copy-done((bf16[2048,512]{1,0:T(8,128)(2,1)S(1)}, bf16[2048,512]{1,0:T(8,128)(2,1)}, u32[]{:S(2)}) %copy-start) | copy-done | bytes 2097176
  4.3 0.0 copy-start.1
  4.3 1.6 %copy-done.1 = bf16[2048,512]{1,0:T(8,128)(2,1)S(1)} copy-done((bf16[2048,512]{1,0:T(8,128)(2,1)S(1)}, bf16[2048,512]{1,0:T(8,128)(2,1)}, u32[]{:S(2)}) %copy-start.1) | copy-done | bytes 2097176
  5.9 0.0 copy-start.6
  5.9 0.9 %copy-done.6 = bf16[24,2048]{1,0:T(8,128)(2,1)S(1)} copy-done((bf16[24,2048]{1,0:T(8,128)(2,1)S(1)}, bf16[24,2048]{1,0:T(8,128)(2,1)}, u32[]{:S(2)}) %copy-start.6) | copy-done | bytes 98328
  6.8 0.0 copy-start.8
  6.8 0.7 %copy-done.8 = f32[2048]{0:T(1024)S(1)} copy-done((f32[2048]{0:T(1024)S(1)}, f32[2048]{0:T(1024)}, u32[]{:S(2)}) %copy-start.8) | copy-done | bytes 8216
  7.5 0.0 copy-start.10
  7.5 0.7 %copy-done.10 = f32[4]{0:T(128)S(1)} copy-done((f32[4]{0:T(128)S(1)}, f32[4]{0:T(128)}, u32[]{:S(2)}) %copy-start.10) | copy-done | bytes 40
  8.1 0.0 copy-start.11
  8.1 0.7 %copy-done.11 = f32[4]{0:T(128)S(1)} copy-done((f32[4]{0:T(128)S(1)}, f32[4]{0:T(128)}, u32[]{:S(2)}) %copy-start.11) | copy-done | bytes 40
  8.8 0.0 copy-start.12
  8.8 0.7 %copy-done.12 = f32[128]{0:T(128)S(1)} copy-done((f32[128]{0:T(128)S(1)}, f32[128]{0:T(128)}, u32[]{:S(2)}) %copy-start.12) | copy-done | bytes 536
  9.4 0.0 copy-start.13
  9.4 0.0 copy-start.14
  9.4 0.0 copy-start.2
  9.5 0.0 copy-start.7
  9.5 0.0 copy-start.9
  9.5 11.5 %mixer.1 = (bf16[24,512]{1,0:T(8,128)(2,1)S(1)}, f32[24,4,128,128]{3,2,1,0:T(8,128)}) custom-call(bf16[24,2048]{1,0:T(8,128)(2,1)S(1)} %copy-done.6, f32[1,2048]{1,0:T(1,128)S(1)} %bitcast.5, bf16[2048,512]{1,0:T(8,128)(2,1)S(1)} %copy-done, bf16[2048,512]{1,0:T(8,128)(2,1)S(1)} %copy-done.1, bf16[2048,512]{1,0:T(8,128)(2,1)} %wv.1, bf16[2048,512]{1,0:T(8,128)(2,1)} %wz.1, ...), custom_call_target="tpu_custom_call" | custom-call | tf_op jit(solution)/shard_map/mixer/pallas_call | solution.py:411
  21.0 0.0 copy-done.13
  21.0 0.1 copy.23.routes
  21.1 0.0 copy-done.14
  21.1 0.1 copy.24.weights
  21.2 0.0 copy-done.2
  21.2 0.0 copy-done.7
  21.2 0.0 copy-done.9
  21.2 0.0 copy-start.3
  21.2 1.2 %copy-done.3 = bf16[1,2048,256]{2,1,0:T(8,128)(2,1)S(1)} copy-done((bf16[1,2048,256]{2,1,0:T(8,128)(2,1)S(1)}, bf16[1,2048,256]{2,1,0:T(8,128)(2,1)}, u32[]{:S(2)}) %copy-start.3) | copy-done | bytes 1048600
  22.4 0.0 copy-start.4
  22.4 1.2 %copy-done.4 = bf16[1,2048,256]{2,1,0:T(8,128)(2,1)S(1)} copy-done((bf16[1,2048,256]{2,1,0:T(8,128)(2,1)S(1)}, bf16[1,2048,256]{2,1,0:T(8,128)(2,1)}, u32[]{:S(2)}) %copy-start.4) | copy-done | bytes 1048600
  23.6 0.0 copy-start.5
  23.6 1.2 %copy-done.5 = bf16[1,256,2048]{2,1,0:T(8,128)(2,1)S(1)} copy-done((bf16[1,256,2048]{2,1,0:T(8,128)(2,1)S(1)}, bf16[1,256,2048]{2,1,0:T(8,128)(2,1)}, u32[]{:S(2)}) %copy-start.5) | copy-done | bytes 1048600
  24.9 25.8 %experts.1 = bf16[24,1024]{1,0:T(8,128)(2,1)S(1)} custom-call(bf16[24,2048]{1,0:T(8,128)(2,1)S(1)} %copy-done.7, bf16[24,512]{1,0:T(8,128)(2,1)S(1)} %get-tuple-element.4.heads_out, bf16[512,2048]{1,0:T(8,128)(2,1)S(1)} %copy-done.2, f32[1,2048]{1,0:T(1,128)S(1)} %bitcast.6, bf16[1,2048,256]{2,1,0:T(8,128)(2,1)S(1)} %copy-done.3, ...), custom_call_target="tpu_custom_call" | custom-call | tf_op jit(solution)/shard_map/experts/pallas_call | solution.py:457
  50.7 0.6 %copy.26 = bf16[24,1024]{1,0:T(8,128)(2,1)} copy(bf16[24,1024]{1,0:T(8,128)(2,1)S(1)} %experts.1) | data formatting | bytes 98304
Async XLA Ops:
  2.7 1.6 %copy-start = (bf16[2048,512]{1,0:T(8,128)(2,1)S(1)}, bf16[2048,512]{1,0:T(8,128)(2,1)}, u32[]{:S(2)}) copy-start(bf16[2048,512]{1,0:T(8,128)(2,1)} %wq.1) | copy-start | bytes 6291460
  4.3 1.6 %copy-start.1 = (bf16[2048,512]{1,0:T(8,128)(2,1)S(1)}, bf16[2048,512]{1,0:T(8,128)(2,1)}, u32[]{:S(2)}) copy-start(bf16[2048,512]{1,0:T(8,128)(2,1)} %wk.1) | copy-start | bytes 6291460
  5.9 0.9 %copy-start.6 = (bf16[24,2048]{1,0:T(8,128)(2,1)S(1)}, bf16[24,2048]{1,0:T(8,128)(2,1)}, u32[]{:S(2)}) copy-start(bf16[24,2048]{1,0:T(8,128)(2,1)} %tokens.3) | copy-start | bytes 294916
  6.8 0.7 %copy-start.8 = (f32[2048]{0:T(1024)S(1)}, f32[2048]{0:T(1024)}, u32[]{:S(2)}) copy-start(f32[2048]{0:T(1024)} %param.20) | copy-start | bytes 24580
  7.5 0.7 %copy-start.10 = (f32[4]{0:T(128)S(1)}, f32[4]{0:T(128)}, u32[]{:S(2)}) copy-start(f32[4]{0:T(128)} %param.27) | copy-start | bytes 52
  8.1 0.7 %copy-start.11 = (f32[4]{0:T(128)S(1)}, f32[4]{0:T(128)}, u32[]{:S(2)}) copy-start(f32[4]{0:T(128)} %param.28) | copy-start | bytes 52
  8.8 0.7 %copy-start.12 = (f32[128]{0:T(128)S(1)}, f32[128]{0:T(128)}, u32[]{:S(2)}) copy-start(f32[128]{0:T(128)} %param.30) | copy-start | bytes 1540
  9.4 11.5 %copy-start.13 = (s32[24,2]{0,1:T(2,128)S(1)}, s32[24,2]{0,1:T(2,128)}, u32[]{:S(2)}) copy-start(s32[24,2]{0,1:T(2,128)} %param.36) | copy-start | bytes 580
  9.4 11.6 %copy-start.14 = (f32[24,2]{0,1:T(2,128)S(1)}, f32[24,2]{0,1:T(2,128)}, u32[]{:S(2)}) copy-start(f32[24,2]{0,1:T(2,128)} %param.37) | copy-start | bytes 580
  9.4 11.7 %copy-start.2 = (bf16[512,2048]{1,0:T(8,128)(2,1)S(1)}, bf16[512,2048]{1,0:T(8,128)(2,1)}, u32[]{:S(2)}) copy-start(bf16[512,2048]{1,0:T(8,128)(2,1)} %w_out.1) | copy-start | bytes 6291460
  9.5 11.7 %copy-start.7 = (bf16[24,2048]{1,0:T(8,128)(2,1)S(1)}, bf16[24,2048]{1,0:T(8,128)(2,1)}, u32[]{:S(2)}) copy-start(bf16[24,2048]{1,0:T(8,128)(2,1)} %tokens.3) | copy-start | bytes 294916
  9.5 11.7 %copy-start.9 = (f32[2048]{0:T(1024)S(1)}, f32[2048]{0:T(1024)}, u32[]{:S(2)}) copy-start(f32[2048]{0:T(1024)} %param.32) | copy-start | bytes 24580
  21.2 1.2 %copy-start.3 = (bf16[1,2048,256]{2,1,0:T(8,128)(2,1)S(1)}, bf16[1,2048,256]{2,1,0:T(8,128)(2,1)}, u32[]{:S(2)}) copy-start(bf16[1,2048,256]{2,1,0:T(8,128)(2,1)} %w_gate.1) | copy-start | bytes 3145732
  22.4 1.2 %copy-start.4 = (bf16[1,2048,256]{2,1,0:T(8,128)(2,1)S(1)}, bf16[1,2048,256]{2,1,0:T(8,128)(2,1)}, u32[]{:S(2)}) copy-start(bf16[1,2048,256]{2,1,0:T(8,128)(2,1)} %w_up.1) | copy-start | bytes 3145732
  23.6 1.2 %copy-start.5 = (bf16[1,256,2048]{2,1,0:T(8,128)(2,1)S(1)}, bf16[1,256,2048]{2,1,0:T(8,128)(2,1)}, u32[]{:S(2)}) copy-start(bf16[1,256,2048]{2,1,0:T(8,128)(2,1)} %w_down.1) | copy-start | bytes 3145732

commit v2 on v1

--- a/solution.py
+++ b/solution.py
@@ -10,7 +10,8 @@
 EPS = 1e-06
 F32 = jnp.float32
 BF16 = jnp.bfloat16
-ANY = pl.BlockSpec(memory_space=pl.ANY)
+VMEM_LIMIT = 60 * 1024 * 1024
+HBM = pl.BlockSpec(memory_space=pltpu.HBM)
 VMEM = pl.BlockSpec(memory_space=pltpu.VMEM)
 
 
@@ -26,22 +27,34 @@
     return x * jax.nn.sigmoid(x)
 
 
+def nt_dot(rows, weight):
+    return lax.dot_general(rows, weight, (((1,), (1,)), ((), ())), preferred_element_type=F32)
+
+
 def mixer_kernel(
     step,
-    tokens,
-    gain,
+    tokens_ref,
+    gain_ref,
     wq,
     wk,
     wv,
     wz,
+    wd_ref,
+    wb_ref,
+    rate_ref,
+    bias_ref,
+    state,
+    out_gain_ref,
+    heads_out,
+    new_state,
+    tokens,
+    gain,
     wd,
     wb,
     rate,
     bias,
-    state,
     out_gain,
-    heads_out,
-    new_state,
+    small_sem,
     wbuf,
     st,
     ns,
@@ -70,19 +83,37 @@
         rows = pl.ds(c * step, step)
         return pltpu.make_async_copy(ns.at[rows], new_state.at[rows], out_sem.at[c])
 
+    small = [
+        pltpu.make_async_copy(src, dst, small_sem.at[n])
+        for n, (src, dst) in enumerate(
+            (
+                (tokens_ref, tokens),
+                (gain_ref, gain),
+                (wd_ref, wd),
+                (wb_ref, wb),
+                (rate_ref, rate),
+                (bias_ref, bias),
+                (out_gain_ref, out_gain),
+            )
+        )
+    ]
+    for copy in small:
+        copy.start()
     for n in range(4):
         w_copy(n).start()
     for c in range(chunks):
         in_copy(c).start()
+    for copy in small:
+        copy.wait()
 
     normed = rms_scale(tokens[...].astype(F32), gain[...]).astype(BF16)
 
     def rounded(weight):
         return jnp.dot(normed, weight, preferred_element_type=F32).astype(BF16).astype(F32)
 
-    xa = rounded(wd[...]) + bias[...]
+    xa = nt_dot(normed, wd[...]).astype(BF16).astype(F32) + bias[...]
     fade = jnp.exp(-rate[...] * (jnp.maximum(xa, 0.0) + jnp.log1p(jnp.exp(-jnp.abs(xa)))))
-    beta = jax.nn.sigmoid(rounded(wb[...]))
+    beta = jax.nn.sigmoid(nt_dot(normed, wb[...]).astype(BF16).astype(F32))
     for h in range(heads):
         fades[:, h, :] = jnp.broadcast_to(fade[:, h : h + 1], (seqs, dim))
         betas[:, h, :] = jnp.broadcast_to(beta[:, h : h + 1], (seqs, dim))
@@ -136,17 +167,23 @@
     n_tp,
     top,
     cap,
+    live,
     groups,
-    tokens,
-    heads_out,
+    tokens_ref,
+    heads_ref,
     w_out,
-    ffn_gain,
+    gain_ref,
     w_gate,
     w_up,
     w_down,
+    routes_ref,
+    weights_ref,
+    out,
+    tokens,
+    heads_out,
+    ffn_gain,
     routes,
     weights,
-    out,
     wo,
     wg,
     wu,
@@ -180,6 +217,7 @@
     e = lax.axis_index("ep")
     t = lax.axis_index("tp")
     u = n_tp - 1 - t
+    used = pl.ds(0, live)
 
     def peer(i):
         return lax.rem(e + i, n_ep)
@@ -201,11 +239,29 @@
     loads = [
         pltpu.make_async_copy(src, dst, w_sem.at[n])
         for n, (src, dst) in enumerate(
-            ((w_out, wo), (w_gate.at[0], wg), (w_up.at[0], wu), (w_down.at[0], wdn))
+            (
+                (heads_ref, heads_out),
+                (w_out, wo),
+                (tokens_ref, tokens),
+                (routes_ref, routes),
+                (weights_ref, weights),
+                (gain_ref, ffn_gain),
+                (w_gate.at[0], wg),
+                (w_up.at[0], wu),
+                (w_down.at[0], wdn),
+            )
         )
     ]
     for load in loads:
         load.start()
+    for n in (2, 3, 4, 5):
+        loads[n].wait()
+    eye = lax.broadcasted_iota(jnp.int32, (seqs, seqs), 1) == lax.broadcasted_iota(
+        jnp.int32, (seqs, seqs), 0
+    )
+
+    def column(row):
+        return jnp.sum(jnp.where(eye, row, 0.0), axis=1, keepdims=True)
 
     lower = (
         lax.broadcasted_iota(jnp.int32, (seqs, seqs), 1)
@@ -214,7 +270,7 @@
     picks = []
     taken = jnp.zeros((1, n_ep), F32)
     for j in range(top):
-        route = routes[:, j : j + 1]
+        route = column(routes[j : j + 1, :].astype(F32)).astype(jnp.int32)
         hot = lax.broadcasted_iota(jnp.int32, (seqs, n_ep), 1) == route
         hot_f = hot.astype(F32)
         before = jnp.dot(lower, hot_f.astype(BF16), preferred_element_type=F32) + taken
@@ -227,6 +283,7 @@
     spread = sum(picks[1:], picks[0]).T.astype(BF16)
 
     loads[0].wait()
+    loads[1].wait()
     part_out[...] = jnp.dot(heads_out[...], wo[...], preferred_element_type=F32).astype(BF16)
     pl.semaphore_wait(barrier, n_ep)
 
@@ -250,8 +307,8 @@
 
     def go(i):
         return pltpu.make_async_remote_copy(
-            src_ref=disp.at[peer(i)],
-            dst_ref=arrived.at[t, e],
+            src_ref=disp.at[peer(i), used],
+            dst_ref=arrived.at[t, e, used],
             send_sem=go_send.at[i],
             recv_sem=go_recv.at[i],
             device_id={"ep": peer(i), "tp": t},
@@ -261,8 +318,8 @@
     def forward(i):
         s = source(i)
         return pltpu.make_async_remote_copy(
-            src_ref=arrived.at[t, s],
-            dst_ref=arrived.at[t, s],
+            src_ref=arrived.at[t, s, used],
+            dst_ref=arrived.at[t, s, used],
             send_sem=fw_send.at[i],
             recv_sem=fw_recv.at[i],
             device_id=partner,
@@ -283,8 +340,8 @@
         return carry
 
     lax.fori_loop(1, n_ep, pass_on, 0)
-    loads[1].wait()
-    loads[2].wait()
+    loads[6].wait()
+    loads[7].wait()
 
     def half(which):
         got = arrived[which].astype(F32).reshape(n_ep * cap, cols).astype(BF16)
@@ -303,7 +360,7 @@
     lax.fori_loop(0, n_ep, fw_done, 0)
     more_g, more_u = half(u)
     hidden = (silu(acc_g[...] + more_g) * (acc_u[...] + more_u)).astype(BF16)
-    loads[3].wait()
+    loads[8].wait()
 
     size = n_ep // groups
 
@@ -321,8 +378,8 @@
     def back(s):
         i = lax.rem(e + n_ep - s, n_ep)
         return pltpu.make_async_remote_copy(
-            src_ref=ret_out.at[s],
-            dst_ref=ret_in.at[e],
+            src_ref=ret_out.at[s, used],
+            dst_ref=ret_in.at[e, used],
             send_sem=back_send.at[i],
             recv_sem=back_recv.at[i],
             device_id={"ep": s, "tp": t},
@@ -357,12 +414,14 @@
         return carry
 
     lax.fori_loop(1, n_ep, back_done, 0)
-    returned = ret_in[...].astype(F32).reshape(n_ep * cap, cols).astype(BF16)
+    kept = lax.broadcasted_iota(jnp.int32, (n_ep, cap, cols), 1) < live
+    returned = jnp.where(kept, ret_in[...].astype(F32), 0.0)
+    returned = returned.reshape(n_ep * cap, cols).astype(BF16)
     total = resid[:, own]
     combined = None
     for j in range(top):
         found = jnp.dot(picks[j].astype(BF16), returned, preferred_element_type=F32)
-        term = found * weights[:, j : j + 1]
+        term = found * column(weights[j : j + 1, :])
         combined = term if combined is None else combined + term
     out[...] = (total + combined).astype(BF16)
 
@@ -414,9 +473,17 @@
             jax.ShapeDtypeStruct((seqs, inner), BF16),
             jax.ShapeDtypeStruct(state.shape, F32),
         ),
-        in_specs=[VMEM, VMEM, ANY, ANY, ANY, ANY, VMEM, VMEM, VMEM, VMEM, ANY, VMEM],
-        out_specs=(VMEM, ANY),
+        in_specs=[HBM] * 12,
+        out_specs=(VMEM, HBM),
         scratch_shapes=[
+            pltpu.VMEM((seqs, width), BF16),
+            pltpu.VMEM((1, width), F32),
+            pltpu.VMEM((heads, width), BF16),
+            pltpu.VMEM((heads, width), BF16),
+            pltpu.VMEM((1, heads), F32),
+            pltpu.VMEM((1, heads), F32),
+            pltpu.VMEM((1, dim), F32),
+            pltpu.SemaphoreType.DMA((7,)),
             pltpu.VMEM((4, width, inner), BF16),
             pltpu.VMEM(state.shape, F32),
             pltpu.VMEM(state.shape, F32),
@@ -431,7 +498,7 @@
             pltpu.SemaphoreType.DMA((chunks,)),
             pltpu.SemaphoreType.DMA((chunks,)),
         ],
-        compiler_params=pltpu.CompilerParams(vmem_limit_bytes=48 * 1024 * 1024),
+        compiler_params=pltpu.CompilerParams(vmem_limit_bytes=VMEM_LIMIT),
         name="mixer",
     )(
         tokens,
@@ -440,26 +507,32 @@
         w_key,
         w_value,
         w_zgate,
-        w_decay,
-        w_beta,
+        w_decay.T,
+        w_beta.T,
         decay_rate.reshape(1, heads),
         decay_bias.reshape(1, heads),
         state,
         out_gain.reshape(1, dim),
     )
 
-    cap = -(-max(2, 2 * seqs * top // n_ep) // 8) * 8
+    live = max(2, 2 * seqs * top // n_ep)
+    cap = -(-live // 8) * 8
     cols = width // n_tp
     ff = expert_gate.shape[2]
     groups = 4 if n_ep % 4 == 0 else 1
     slots = (n_ep, cap, cols)
     dma = pltpu.SemaphoreType.DMA
     layer_out = pl.pallas_call(
-        functools.partial(expert_kernel, n_ep, n_tp, top, cap, groups),
+        functools.partial(expert_kernel, n_ep, n_tp, top, cap, live, groups),
         out_shape=jax.ShapeDtypeStruct((seqs, cols), BF16),
-        in_specs=[VMEM, VMEM, ANY, VMEM, ANY, ANY, ANY, VMEM, VMEM],
+        in_specs=[HBM] * 9,
         out_specs=VMEM,
         scratch_shapes=[
+            pltpu.VMEM((seqs, width), BF16),
+            pltpu.VMEM((seqs, inner), BF16),
+            pltpu.VMEM((1, width), F32),
+            pltpu.VMEM((top, seqs), jnp.int32),
+            pltpu.VMEM((top, seqs), F32),
             pltpu.VMEM((inner, width), BF16),
             pltpu.VMEM((width, ff), BF16),
             pltpu.VMEM((width, ff), BF16),
@@ -477,7 +550,7 @@
             pltpu.VMEM(slots, BF16),
             pltpu.VMEM(slots, BF16),
             pltpu.VMEM(slots, BF16),
-            dma((4,)),
+            dma((9,)),
             dma((2,)),
             dma((n_ep,)),
             dma((n_ep,)),
@@ -489,7 +562,7 @@
             dma((n_ep,)),
         ],
         compiler_params=pltpu.CompilerParams(
-            collective_id=0, has_side_effects=True, vmem_limit_bytes=48 * 1024 * 1024
+            collective_id=0, has_side_effects=True, vmem_limit_bytes=VMEM_LIMIT
         ),
         name="experts",
     )(
@@ -500,8 +573,8 @@
         expert_gate,
         expert_up,
         expert_down,
-        routes,
-        route_weight,
+        routes.T,
+        route_weight.T,
     )
     return (layer_out, new_state)
 

time: 51.8 us -> 41.3 us (0.80)
  local copies, waits for them, and re-layouts: 13.3 us -> 1.42 us
  Pallas kernels: 37.3 us -> 39.1 us
    unnamed x35 -> x1, local copies, waits for them, and re-layouts: 13.3 us -> 1.42 us
    pallas_call x1, Pallas kernels: 11.5 us -> 14.1 us  [per_device(): pl.pallas_call(functools.partial(mixer_kernel, step), out_shape=(jax.Shap...]
    pallas_call x1, Pallas kernels: 25.8 us -> 25 us  [per_device(): pl.pallas_call(functools.partial(expert_kernel, n_ep, n_tp, top, cap, liv...]
where the time goes in v2:
time: 41.3 us; the launch traced here: 41.2 us
  Pallas kernels  39.1 us (95%)
  local copies, waits for them, and re-layouts  1.42 us (3%)
  between operations  0.65 us (2%)
    pallas_call x1, Pallas kernels, per_device(): pl.pallas_call(functools.partial(expert_kernel, n_ep, n_tp, top, cap, liv...  25 us
    pallas_call x1, Pallas kernels, per_device(): pl.pallas_call(functools.partial(mixer_kernel, step), out_shape=(jax.Shap...  14.1 us
    unnamed x1, local copies, waits for them, and re-layouts  1.42 us

profile of v2, /device:TPU:0, one launch (start us, length us, event | category | flops | bytes accessed | tf_op | source)
XLA Modules:
  0.0 41.2 jit_solution(395506302857668962)
XLA Ops:
  0.6 14.1 %mixer.1 = (bf16[24,512]{1,0:T(8,128)(2,1)}, f32[24,4,128,128]{3,2,1,0:T(8,128)}) custom-call(bf16[24,2048]{1,0:T(8,128)(2,1)} %tokens_ref.3, f32[1,2048]{1,0:T(1,128)} %bitcast.11, bf16[2048,512]{1,0:T(8,128)(2,1)} %wq.1, bf16[2048,512]{1,0:T(8,128)(2,1)} %wk.1, bf16[2048,512]{1,0:T(8,128)(2,1)} %wv.1, bf16[2048,512]{1,0:T(8,128)(2,1)} %wz.1, ...), custom_call_target="tpu_custom_call" | custom-call | tf_op jit(solution)/shard_map/mixer/pallas_call | solution.py:470
  14.7 25.0 %experts.1 = bf16[24,1024]{1,0:T(8,128)(2,1)} custom-call(bf16[24,2048]{1,0:T(8,128)(2,1)} %tokens_ref.3, bf16[24,512]{1,0:T(8,128)(2,1)} %get-tuple-element.4.heads_ref, bf16[512,2048]{1,0:T(8,128)(2,1)} %w_out.1, f32[1,2048]{1,0:T(1,128)} %bitcast.12, bf16[1,2048,256]{2,1,0:T(8,128)(2,1)} %w_gate.1, bf16[1,2048,256]{2,1,0:T(8,128)(2,1)} %w_up.1, ...), custom_call_target="tpu_custom_call" | custom-call | tf_op jit(solution)/shard_map/experts/pallas_call | solution.py:525
  39.7 1.4 %copy.22 = bf16[24,1024]{1,0:T(8,128)(2,1)} copy(bf16[24,1024]{1,0:T(8,128)(2,1)} %experts.1) | data formatting | bytes 98304

commit v3 on v2

--- a/solution.py
+++ b/solution.py
@@ -170,7 +170,7 @@
     live,
     groups,
     tokens_ref,
-    heads_ref,
+    heads_out,
     w_out,
     gain_ref,
     w_gate,
@@ -180,7 +180,6 @@
     weights_ref,
     out,
     tokens,
-    heads_out,
     ffn_gain,
     routes,
     weights,
@@ -240,7 +239,6 @@
         pltpu.make_async_copy(src, dst, w_sem.at[n])
         for n, (src, dst) in enumerate(
             (
-                (heads_ref, heads_out),
                 (w_out, wo),
                 (tokens_ref, tokens),
                 (routes_ref, routes),
@@ -254,7 +252,7 @@
     ]
     for load in loads:
         load.start()
-    for n in (2, 3, 4, 5):
+    for n in (1, 2, 3, 4):
         loads[n].wait()
     eye = lax.broadcasted_iota(jnp.int32, (seqs, seqs), 1) == lax.broadcasted_iota(
         jnp.int32, (seqs, seqs), 0
@@ -283,7 +281,6 @@
     spread = sum(picks[1:], picks[0]).T.astype(BF16)
 
     loads[0].wait()
-    loads[1].wait()
     part_out[...] = jnp.dot(heads_out[...], wo[...], preferred_element_type=F32).astype(BF16)
     pl.semaphore_wait(barrier, n_ep)
 
@@ -340,8 +337,8 @@
         return carry
 
     lax.fori_loop(1, n_ep, pass_on, 0)
+    loads[5].wait()
     loads[6].wait()
-    loads[7].wait()
 
     def half(which):
         got = arrived[which].astype(F32).reshape(n_ep * cap, cols).astype(BF16)
@@ -360,7 +357,7 @@
     lax.fori_loop(0, n_ep, fw_done, 0)
     more_g, more_u = half(u)
     hidden = (silu(acc_g[...] + more_g) * (acc_u[...] + more_u)).astype(BF16)
-    loads[8].wait()
+    loads[7].wait()
 
     size = n_ep // groups
 
@@ -470,7 +467,7 @@
     heads_out, new_state = pl.pallas_call(
         functools.partial(mixer_kernel, step),
         out_shape=(
-            jax.ShapeDtypeStruct((seqs, inner), BF16),
+            pltpu.VMEM((seqs, inner), BF16),
             jax.ShapeDtypeStruct(state.shape, F32),
         ),
         in_specs=[HBM] * 12,
@@ -524,12 +521,11 @@
     dma = pltpu.SemaphoreType.DMA
     layer_out = pl.pallas_call(
         functools.partial(expert_kernel, n_ep, n_tp, top, cap, live, groups),
-        out_shape=jax.ShapeDtypeStruct((seqs, cols), BF16),
-        in_specs=[HBM] * 9,
+        out_shape=pltpu.VMEM((seqs, cols), BF16),
+        in_specs=[HBM, VMEM] + [HBM] * 7,
         out_specs=VMEM,
         scratch_shapes=[
             pltpu.VMEM((seqs, width), BF16),
-            pltpu.VMEM((seqs, inner), BF16),
             pltpu.VMEM((1, width), F32),
             pltpu.VMEM((top, seqs), jnp.int32),
             pltpu.VMEM((top, seqs), F32),
@@ -550,7 +546,7 @@
             pltpu.VMEM(slots, BF16),
             pltpu.VMEM(slots, BF16),
             pltpu.VMEM(slots, BF16),
-            dma((9,)),
+            dma((8,)),
             dma((2,)),
             dma((n_ep,)),
             dma((n_ep,)),
@@ -562,12 +558,12 @@
             dma((n_ep,)),
         ],
         compiler_params=pltpu.CompilerParams(
-            collective_id=0, has_side_effects=True, vmem_limit_bytes=VMEM_LIMIT
+            collective_id=0, has_side_effects=True, vmem_limit_bytes=VMEM_LIMIT - 2**21
         ),
         name="experts",
     )(
         tokens,
-        heads_out,
+        pltpu.with_memory_space_constraint(heads_out, pltpu.VMEM),
         w_out,
         ffn_gain.reshape(1, width),
         expert_gate,

time: 41.3 us -> 39.3 us (0.952)
  Pallas kernels: 39.1 us -> 37.9 us
  local copies, waits for them, and re-layouts: 1.42 us -> 0.62 us
    unnamed x1, local copies, waits for them, and re-layouts: 1.42 us -> 0.62 us
    pallas_call x1, Pallas kernels: 25 us -> 24.4 us  [per_device(): pl.pallas_call(functools.partial(expert_kernel, n_ep, n_tp, top, cap, liv...]
    pallas_call x1, Pallas kernels: 14.1 us -> 13.5 us  [per_device(): pl.pallas_call(functools.partial(mixer_kernel, step), out_shape=(pltpu.VM...]
where the time goes in v3:
time: 39.3 us; the launch traced here: 39.2 us
  Pallas kernels  37.9 us (96%)
  between operations  0.65 us (2%)
  local copies, waits for them, and re-layouts  0.62 us (2%)
    pallas_call x1, Pallas kernels, per_device(): pl.pallas_call(functools.partial(expert_kernel, n_ep, n_tp, top, cap, liv...  24.4 us
    pallas_call x1, Pallas kernels, per_device(): pl.pallas_call(functools.partial(mixer_kernel, step), out_shape=(pltpu.VM...  13.5 us

profile of v3, /device:TPU:0, one launch (start us, length us, event | category | flops | bytes accessed | tf_op | source)
XLA Modules:
  0.0 39.2 jit_solution(16311722495002985502)
XLA Ops:
  0.6 13.5 %mixer.1 = (bf16[24,512]{1,0:T(8,128)(2,1)S(1)}, f32[24,4,128,128]{3,2,1,0:T(8,128)}) custom-call(bf16[24,2048]{1,0:T(8,128)(2,1)} %tokens_ref.3, f32[1,2048]{1,0:T(1,128)} %bitcast.11, bf16[2048,512]{1,0:T(8,128)(2,1)} %wq.1, bf16[2048,512]{1,0:T(8,128)(2,1)} %wk.1, bf16[2048,512]{1,0:T(8,128)(2,1)} %wv.1, bf16[2048,512]{1,0:T(8,128)(2,1)} %wz.1, ...), custom_call_target="tpu_custom_call" | custom-call | tf_op jit(solution)/shard_map/mixer/pallas_call | solution.py:467
  14.1 24.4 %experts.1 = bf16[24,1024]{1,0:T(8,128)(2,1)S(1)} custom-call(bf16[24,2048]{1,0:T(8,128)(2,1)} %tokens_ref.3, bf16[24,512]{1,0:T(8,128)(2,1)S(1)} %get-tuple-element.4.heads_out, bf16[512,2048]{1,0:T(8,128)(2,1)} %w_out.1, f32[1,2048]{1,0:T(1,128)} %bitcast.12, bf16[1,2048,256]{2,1,0:T(8,128)(2,1)} %w_gate.1, bf16[1,2048,256]{2,1,0:T(8,128)(2,1)} %w_up.1, ...), custom_call_target="tpu_custom_call" | custom-call | tf_op jit(solution)/shard_map/experts/pallas_call | solution.py:522
  38.6 0.6 %copy.22 = bf16[24,1024]{1,0:T(8,128)(2,1)} copy(bf16[24,1024]{1,0:T(8,128)(2,1)S(1)} %experts.1) | data formatting | bytes 98304
